TPU v7x, 32 devices: a whole 2x2x4 slice. The times are simulated.
32 devices in a mesh: grp: 2 (over y), fs: 4 (over z), tp: 4 (over x, core).
Axes of the slice: x: 2, y: 2, z: 4, core: 2. Of those that a mesh axis runs over, the one named last changes fastest.
Arguments:
- tokens: bfloat16 [4096, 2048], P(('grp', 'fs'), 'tp'), parts along dimension 0, may hold values from -36 to 36
- query_matrix: bfloat16 [2048, 1024], P('fs', 'tp'), may hold values from -0.125 to 0.125
- key_weight: bfloat16 [2048, 1024], P('fs', 'tp'), may hold values from -0.125 to 0.125
- value_weight: bfloat16 [2048, 2048], P('fs', 'tp'), may hold values from -0.125 to 0.125
- forget_lower_factor: bfloat16 [2048, 32], replicated, may hold values from -0.125 to 0.125
- decay_up: bfloat16 [32, 1024], replicated, may hold values from -1 to 1
- decay_bias: float32 [1024], replicated, may hold values from -1 to 8
- log_extra: float32 [4096, 1024], P(('grp', 'fs'), 'tp'), parts along dimension 0, may hold values from -0.7 to 0
- head_gain: float32 [256], replicated, may hold values from 0.1 to 1.9
- out_weight: bfloat16 [2048, 2048], P('tp', 'fs'), may hold values from -0.125 to 0.125
- mix_gain: float32 [2048], P('tp'), may hold values from 0.1 to 1.9
- up_weight: bfloat16 [2048, 8192], P('fs', 'tp'), may hold values from -0.125 to 0.125
- down_weight: bfloat16 [8192, 2048], P('tp', 'fs'), may hold values from -0.0625 to 0.0625
- out_gain: float32 [2048], P('tp'), may hold values from 0.1 to 1.9
Outputs:
- layer_out: bfloat16 [4096, 2048], P(('grp', 'fs'), 'tp'), parts along dimension 0
There are 2 independent parts, one for each index of `grp`. A program takes and returns all parts, laid end to end along the dimension named above; an argument that names none is the same for every part. Nothing has to cross between parts.
All inputs are finite; a program needn't handle non-finite values.
Results may differ from a plain program's by a relative error of at most 0.015.
Values may be sent and summed in bfloat16 or wider, within the bound.
A program may use at most 64 MiB of HBM per device.

v0:
```python
import jax
import jax.numpy as jnp
from jax import lax
from jax.sharding import PartitionSpec as P

D = 2048
DK = 128
DV = 256
SEGMENT_LENGTH = 64
ALPHA = 2.0**0.5
TAU = 16.0
EPS = 1e-05
HIGH = lax.Precision.HIGHEST


def block_scan(queries, key_rows, value_rows, log_decay):
    span = queries.shape[2]
    causal = (jnp.arange(span)[:, None] >= jnp.arange(span)[None, :])[:, :, None]

    def step(state, inputs):
        query_block, key_block, value_block, decay_block = inputs
        cumul = jnp.cumsum(decay_block, axis=1)
        last_cum = cumul[:, -1:, :]
        carried = jnp.einsum("hcd,hde->hce", query_block * jnp.exp(cumul), state, precision=HIGH)
        differ = cumul[:, :, None, :] - cumul[:, None, :, :]
        weights = jnp.exp(jnp.where(causal, differ, -jnp.inf))
        scores = jnp.sum(query_block[:, :, None, :] * key_block[:, None, :, :] * weights, axis=-1)
        within = jnp.einsum("hij,hje->hie", scores, value_block, precision=HIGH)
        fresh = jnp.einsum(
            "hcd,hce->hde", key_block * jnp.exp(last_cum - cumul), value_block, precision=HIGH
        )
        new_state = jnp.exp(last_cum[:, 0, :])[:, :, None] * state + fresh
        return (new_state, carried + within)

    start = jnp.zeros((queries.shape[1], queries.shape[3], value_rows.shape[3]), jnp.float32)
    _, outputs = lax.scan(step, start, (queries, key_rows, value_rows, log_decay))
    return outputs


def layer_norm(summed, gain_cols):
    row_total, row_squares = lax.psum(
        (jnp.sum(summed, axis=1), jnp.sum(summed * summed, axis=1)), "tp"
    )
    row_mean = row_total / D
    row_var = row_squares / D - row_mean * row_mean
    centered = summed - row_mean[:, None]
    return (centered * lax.rsqrt(row_var[:, None] + EPS) * gain_cols).astype(jnp.bfloat16)


def local(
    tokens,
    query_matrix,
    key_weight,
    value_weight,
    forget_lower_factor,
    decay_up,
    decay_bias,
    log_extra,
    head_gain,
    out_weight,
    mix_gain,
    up_weight,
    down_weight,
    out_gain,
):
    gathered = lax.all_gather(tokens, "tp", axis=1, tiled=True)
    row_count = gathered.shape[0]
    key_cols = query_matrix.shape[1]
    value_cols = value_weight.shape[1]
    local_heads = key_cols // DK
    block_pieces = (
        lax.all_gather(query_matrix, "fs", axis=0, tiled=True),
        lax.all_gather(key_weight, "fs", axis=0, tiled=True),
        lax.all_gather(value_weight, "fs", axis=0, tiled=True),
    )
    columns = gathered
    queries, key_rows, value_rows = tuple(
        (
            jnp.dot(columns, shard_piece, preferred_element_type=jnp.float32)
            for shard_piece in block_pieces
        )
    )
    queries = queries.astype(jnp.bfloat16)
    key_rows = key_rows.astype(jnp.bfloat16)
    value_rows = value_rows.astype(jnp.bfloat16)
    low = jnp.dot(gathered, forget_lower_factor, preferred_element_type=jnp.float32).astype(
        jnp.bfloat16
    )
    offset_cols = lax.axis_index("tp") * key_cols
    local_up = lax.dynamic_slice_in_dim(decay_up, offset_cols, key_cols, 1)
    local_bias = lax.dynamic_slice_in_dim(decay_bias, offset_cols, key_cols, 0)
    gate_pre = jnp.dot(low, local_up, preferred_element_type=jnp.float32) + local_bias
    log_decay = jax.nn.log_sigmoid(gate_pre) / TAU + log_extra
    count = row_count // SEGMENT_LENGTH

    def blocks(array, depth):
        return (
            array.astype(jnp.float32)
            .reshape(count, SEGMENT_LENGTH, local_heads, depth)
            .transpose(0, 2, 1, 3)
        )

    attended = block_scan(
        blocks(queries, DK) * DK ** (-0.5),
        blocks(key_rows, DK),
        blocks(value_rows, DV),
        blocks(log_decay, DK),
    )
    attended = attended.transpose(0, 2, 1, 3).reshape(row_count, local_heads, DV)
    scaled = (
        attended
        * lax.rsqrt(jnp.mean(attended * attended, axis=-1, keepdims=True) + EPS)
        * head_gain
    )
    mixed_heads = scaled.reshape(row_count, value_cols).astype(jnp.bfloat16)
    mix_terms = jnp.dot(
        mixed_heads,
        lax.all_gather(out_weight, "fs", axis=1, tiled=True),
        preferred_element_type=jnp.float32,
    )
    mix = lax.psum_scatter(
        mix_terms.astype(jnp.bfloat16), "tp", scatter_dimension=1, tiled=True
    ).astype(jnp.float32)
    normed_local = layer_norm(ALPHA * tokens.astype(jnp.float32) + mix, mix_gain)
    normed_rows = lax.all_gather(normed_local, "tp", axis=1, tiled=True)
    columns = normed_rows
    hidden = jnp.dot(
        columns,
        lax.all_gather(up_weight, "fs", axis=0, tiled=True),
        preferred_element_type=jnp.float32,
    )
    activation = jnp.square(jax.nn.relu(hidden)).astype(jnp.bfloat16)
    down_terms = jnp.dot(
        activation,
        lax.all_gather(down_weight, "fs", axis=1, tiled=True),
        preferred_element_type=jnp.float32,
    )
    down = lax.psum_scatter(
        down_terms.astype(jnp.bfloat16), "tp", scatter_dimension=1, tiled=True
    ).astype(jnp.float32)
    return layer_norm(ALPHA * normed_local.astype(jnp.float32) + down, out_gain)


def solution(mesh):
    in_specs = (
        P(("grp", "fs"), "tp"),
        P("fs", "tp"),
        P("fs", "tp"),
        P("fs", "tp"),
        P(),
        P(),
        P(),
        P(("grp", "fs"), "tp"),
        P(),
        P("tp", "fs"),
        P("tp"),
        P("fs", "tp"),
        P("tp", "fs"),
        P("tp"),
    )
    out_specs = P(("grp", "fs"), "tp")
    return jax.shard_map(local, mesh=mesh, in_specs=in_specs, out_specs=out_specs, check_vma=False)
```

profile of v0, /device:TPU:0, one launch (start us, length us, event | category | flops | bytes accessed | tf_op | source)
XLA Modules:
  0.0 615.8 jit_solution(9214274555413043903)
XLA Ops:
  6.5 0.7 all-gather.9.cloned.1.call-update
  7.3 0.7 all-gather.15.cloned.1.call-update
  8.1 0.7 all-gather.11.cloned.1.call-update
  8.8 0.5 all-gather.13.cloned.1.call-update
  9.4 0.5 all-gather.17.cloned.1.call-update
  10.0 0.8 dynamic_slice.21
  10.8 23.4 %all-gather.9.cloned.1.call-done = bf16[512,2048]{1,0:T(8,128)(2,1)} async-done(((bf16[512,512]{1,0:T(8,128)(2,1)}), bf16[512,2048]{1,0:T(8,128)(2,1)}) %all-gather.9.cloned.1.call-update) | async-done | bytes 2097168 | tf_op jit(solution)/shard_map/all_gather | solution.py:66
  34.2 2.8 fusion.31
  37.3 0.9 copy.64
  38.1 25.7 %all-gather.15.cloned.1.call-done = bf16[2048,256]{1,0:T(8,128)(2,1)} async-done(((bf16[512,256]{1,0:T(8,128)(2,1)}), bf16[2048,256]{1,0:T(8,128)(2,1)}) %all-gather.15.cloned.1.call-update) | async-done | bytes 1048592 | tf_op jit(solution)/shard_map/all_gather | solution.py:72
  63.8 2.6 fusion.26
  66.4 1.1 mul.127
  67.4 25.3 %all-gather.11.cloned.1.call-done = bf16[2048,256]{1,0:T(8,128)(2,1)} async-done(((bf16[512,256]{1,0:T(8,128)(2,1)}), bf16[2048,256]{1,0:T(8,128)(2,1)}) %all-gather.11.cloned.1.call-update) | async-done | bytes 1048592 | tf_op jit(solution)/shard_map/all_gather | solution.py:73
  92.8 2.6 fusion.24
  95.3 1.1 reshape.84
  96.4 42.9 %all-gather.13.cloned.1.call-done = bf16[2048,512]{1,0:T(8,128)(2,1)} async-done(((bf16[512,512]{1,0:T(8,128)(2,1)}), bf16[2048,512]{1,0:T(8,128)(2,1)}) %all-gather.13.cloned.1.call-update) | async-done | bytes 2097168 | tf_op jit(solution)/shard_map/all_gather | solution.py:74
  139.3 3.5 fusion.22
  142.7 0.7 reshape.85
  143.6 0.9 copy-done.3
  144.6 0.9 copy_bitcast_fusion.1
  145.6 38.5 %while.13 = (s32[]{:T(128)}, f32[2,128,256]{2,1,0:T(8,128)S(1)}, f32[8,2,64,256]{3,2,1,0:T(8,128)S(1)}, f32[8,2,64,128]{3,2,1,0:T(8,128)}, f32[8,2,64,128]{3,2,1...) while((s32[]{:T(128)}, f32[2,128,256]{2,1,0:T(8,128)S(1)}, ...), condition=%wide.region_3.4_spmd.clone, body=%wide.region_0.3_spmd.clone.sunk | while | flops 132444160 | bytes 2539644 | solution.py:36
  145.6 0.9 dynamic-slice_bitcast_fusion.7
  146.4 0.9 dynamic-slice_bitcast_fusion.6
  147.4 1.9 multiply_reduce_fusion.5
  150.4 0.9 dynamic-slice_bitcast_fusion.7
  151.2 0.9 dynamic-slice_bitcast_fusion.6
  152.2 1.9 multiply_reduce_fusion.5
  154.7 0.4 convolution_add_fusion.4
  155.2 0.9 dynamic-slice_bitcast_fusion.7
  156.1 0.9 dynamic-slice_bitcast_fusion.6
  157.0 1.9 multiply_reduce_fusion.5
  160.0 0.9 dynamic-slice_bitcast_fusion.7
  160.9 0.9 dynamic-slice_bitcast_fusion.6
  161.8 1.9 multiply_reduce_fusion.5
  164.8 0.9 dynamic-slice_bitcast_fusion.7
  165.7 0.9 dynamic-slice_bitcast_fusion.6
  166.7 1.9 multiply_reduce_fusion.5
  169.7 0.9 dynamic-slice_bitcast_fusion.7
  170.5 0.9 dynamic-slice_bitcast_fusion.6
  171.5 1.9 multiply_reduce_fusion.5
  174.5 0.9 dynamic-slice_bitcast_fusion.7
  175.3 0.9 dynamic-slice_bitcast_fusion.6
  176.3 1.9 multiply_reduce_fusion.5
  178.8 0.4 convolution_add_fusion.4
  179.3 0.9 dynamic-slice_bitcast_fusion.7
  180.2 0.9 dynamic-slice_bitcast_fusion.6
  181.1 1.9 multiply_reduce_fusion.5
  184.5 0.6 mul.130
  185.2 0.8 copy.47
  186.1 4.2 convolution_convert_fusion.1
  190.4 30.1 %reduce-scatter.3.cloned.1.call-done = bf16[512,512]{1,0:T(8,128)(2,1)} async-done(((bf16[512,2048]{1,0:T(8,128)(2,1)}), bf16[512,512]{1,0:T(8,128)(2,1)}) %reduce-scatter.3.cloned.1.call-update) | async-done | bytes 524304 | tf_op jit(solution)/shard_map/reduce_scatter | solution.py:121
  220.4 1.4 fusion.27
  221.8 5.8 all-reduce.1
  227.6 2.1 multiply_convert_fusion.2
  229.8 0.7 all-gather.21.cloned.1.call-update
  230.5 0.7 all-gather.23.cloned.1.call-update
  231.4 21.6 %all-gather.19.cloned.1.call-done = bf16[512,2048]{1,0:T(8,128)(2,1)} async-done(((bf16[512,512]{1,0:T(8,128)(2,1)}), bf16[512,2048]{1,0:T(8,128)(2,1)}) %all-gather.19.cloned.1.call-update) | async-done | bytes 2097168 | tf_op jit(solution)/shard_map/all_gather | solution.py:125
  253.1 151.2 %all-gather.21.cloned.1.call-done = bf16[2048,2048]{1,0:T(8,128)(2,1)} async-done(((bf16[512,2048]{1,0:T(8,128)(2,1)}), bf16[2048,2048]{1,0:T(8,128)(2,1)}) %all-gather.21.cloned.1.call-update) | async-done | bytes 8388624 | tf_op jit(solution)/shard_map/all_gather | solution.py:129
  404.3 149.4 %all-gather.23.cloned.1.call-done = bf16[2048,2048]{1,0:T(8,128)(2,1)} async-done(((bf16[2048,512]{1,0:T(8,128)(2,1)}), bf16[2048,2048]{1,0:T(8,128)(2,1)}) %all-gather.23.cloned.1.call-update) | async-done | bytes 8388624 | tf_op jit(solution)/shard_map/all_gather | solution.py:135
  553.7 16.5 %convolution_convert_fusion = bf16[512,2048]{1,0:T(8,128)(2,1)} fusion(bf16[2048,2048]{1,0:T(8,128)(2,1)} %all-gather.23.cloned.1.call-done, bf16[512,2048]{1,0:T(8,128)(2,1)} %all-gather.19.cloned.1.call-done, bf16[2048,2048]{1,0:T(8,128)(2,1)} %all-gather.21.cloned.1.call-done), kind=kOutput, calls=%fused_computation.29 | convolution fusion | flops 8594128896 | bytes 20971520 | tf_op jit(solution)/shard_map/dot_general | solution.py:133
  570.2 29.5 %reduce-scatter.5.cloned.1.call-done = bf16[512,512]{1,0:T(8,128)(2,1)} async-done(((bf16[512,2048]{1,0:T(8,128)(2,1)}), bf16[512,512]{1,0:T(8,128)(2,1)}) %reduce-scatter.5.cloned.1.call-update) | async-done | bytes 524304 | tf_op jit(solution)/shard_map/reduce_scatter | solution.py:138
  599.7 1.4 fusion.28
  601.1 5.8 all-reduce
  606.9 2.1 multiply_convert_fusion.1
  (98 shorter events, 9.6 us)
Async XLA Ops:
  6.5 27.7 %copy-start = (bf16[2048,32]{0,1:T(8,128)(2,1)S(1)}, bf16[2048,32]{0,1:T(8,128)(2,1)}, u32[]{:S(2)}) copy-start(bf16[2048,32]{0,1:T(8,128)(2,1)} %param.20) | copy-start | bytes 393220
  6.5 3.4 copy-start.7
  6.5 27.7 %copy-start.8 = (f32[512,256]{1,0:T(8,128)S(1)}, f32[512,256]{1,0:T(8,128)}, u32[]{:S(2)}) copy-start(f32[512,256]{1,0:T(8,128)} %param.23) | copy-start | bytes 1572868
  6.5 27.7 %all-gather.9.cloned.1.call-start = ((), (), s32[]{:S(2)}) async-start(), calls=%async_computation.2 | async-start | bytes 2621440 | tf_op jit(solution)/shard_map/all_gather | solution.py:66
  7.3 56.5 %all-gather.15.cloned.1.call-start = ((), (), s32[]{:S(2)}) async-start(), calls=%async_computation.5 | async-start | bytes 1310720 | tf_op jit(solution)/shard_map/all_gather | solution.py:72
  8.0 84.8 %all-gather.11.cloned.1.call-start = ((), (), s32[]{:S(2)}) async-start(), calls=%async_computation.3 | async-start | bytes 1310720 | tf_op jit(solution)/shard_map/all_gather | solution.py:73
  8.7 130.5 %all-gather.13.cloned.1.call-start = ((), (), s32[]{:S(2)}) async-start(), calls=%async_computation.4 | async-start | bytes 2621440 | tf_op jit(solution)/shard_map/all_gather | solution.py:74
  9.3 176.8 %all-gather.17.cloned.1.call-start = ((), (), s32[]{:S(2)}) async-start(), calls=%async_computation.6 | async-start | bytes 2621440 | tf_op jit(solution)/shard_map/all_gather | solution.py:118
  9.9 210.5 %reduce-scatter.3.cloned.1.call-start = ((), (), s32[]{:S(2)}) async-start(), calls=%async_computation.7 | async-start | bytes 2621440 | tf_op jit(solution)/shard_map/reduce_scatter | solution.py:121
  143.4 1.0 copy-start.3
  143.4 1.2 copy-start.4
  190.3 30.1 %copy-start.2 = (bf16[512,512]{1,0:T(8,128)(2,1)S(1)}, bf16[512,512]{1,0:T(8,128)(2,1)}, u32[]{:S(2)}) copy-start(bf16[512,512]{1,0:T(8,128)(2,1)} %param.16) | copy-start | bytes 1572868
  190.3 37.3 %copy-start.5 = (f32[512]{0:T(512)S(1)}, f32[512]{0:T(512)}, u32[]{:S(2)}) copy-start(f32[512]{0:T(512)} %param.26) | copy-start | bytes 6148
  190.3 62.7 %all-gather.19.cloned.1.call-start = ((), (), s32[]{:S(2)}) async-start(), calls=%async_computation.8 | async-start | bytes 2621440 | tf_op jit(solution)/shard_map/all_gather | solution.py:125
  229.7 174.6 %all-gather.21.cloned.1.call-start = ((), (), s32[]{:S(2)}) async-start(), calls=%async_computation.9 | async-start | bytes 10485760 | tf_op jit(solution)/shard_map/all_gather | solution.py:129
  230.5 323.2 %all-gather.23.cloned.1.call-start = ((), (), s32[]{:S(2)}) async-start(), calls=%async_computation.10 | async-start | bytes 10485760 | tf_op jit(solution)/shard_map/all_gather | solution.py:135
  231.2 368.5 %reduce-scatter.5.cloned.1.call-start = ((), (), s32[]{:S(2)}) async-start(), calls=%async_computation.11 | async-start | bytes 2621440 | tf_op jit(solution)/shard_map/reduce_scatter | solution.py:138
  570.2 29.5 %copy-start.1 = (bf16[512,512]{1,0:T(8,128)(2,1)S(1)}, bf16[512,512]{1,0:T(8,128)(2,1)}, u32[]{:S(2)}) copy-start(bf16[512,512]{1,0:T(8,128)(2,1)} %multiply_convert_fusion.2) | copy-start | bytes 1572868
  570.2 36.7 %copy-start.6 = (f32[512]{0:T(512)S(1)}, f32[512]{0:T(512)}, u32[]{:S(2)}) copy-start(f32[512]{0:T(512)} %param.29) | copy-start | bytes 6148
Sparse Core Ops, SparseCore 0:
  8.9 25.2 all-gather.8
  35.8 27.9 all-gather.14
  65.4 27.3 all-gather.10
  94.2 45.0 all-gather.12
  140.7 44.4 all-gather.16
  190.4 29.9 reduce-scatter.2
  229.8 23.1 all-gather.18
  254.6 149.6 all-gather.20
  405.8 147.7 all-gather.22
  570.3 29.3 reduce-scatter.4
where the time goes:
time: 617 us; the launch traced here: 616 us
  waiting for transfers between devices  504 us (82%)
  matrix products  39.9 us (6%)
  other arithmetic  23.6 us (4%)
  local copies, waits for them, and re-layouts  22.3 us (4%)
  between operations  13.7 us (2%)
  blocking collectives  11.5 us (2%)
    all_gather x1, waiting for transfers between devices, local(): lax.all_gather(up_weight, 'fs', axis=0, tiled=True)  151 us
    all_gather x1, waiting for transfers between devices, local(): lax.all_gather(down_weight, 'fs', axis=1, tiled=True)  149 us
    all_gather x1, waiting for transfers between devices, local(): lax.all_gather(value_weight, 'fs', axis=0, tiled=True)  42.9 us
    reduce_scatter x1, waiting for transfers between devices, local(): lax.psum_scatter(mix_terms.astype(jnp.bfloat16), 'tp', scatter_dimension=...  30.1 us
    reduce_scatter x1, waiting for transfers between devices, local(): lax.psum_scatter(down_terms.astype(jnp.bfloat16), 'tp', scatter_dimension...  29.5 us
    all_gather x1, waiting for transfers between devices, local(): lax.all_gather(query_matrix, 'fs', axis=0, tiled=True)  25.7 us
    all_gather x1, waiting for transfers between devices, local(): lax.all_gather(key_weight, 'fs', axis=0, tiled=True)  25.3 us
    all_gather x1, waiting for transfers between devices, local(): gathered = lax.all_gather(tokens, 'tp', axis=1, tiled=True)  23.4 us
  transfers between devices with their start and end apart: 10, of which 9 were waited for; matrix products, arithmetic and copies ran while one was open for 9% of the time, Pallas kernels for 0%

commit v1 on v0

--- a/solution.py
+++ b/solution.py
@@ -1,3 +1,4 @@
+import functools
 import jax
 import jax.numpy as jnp
 from jax import lax
@@ -11,6 +12,22 @@
 TAU = 16.0
 EPS = 1e-05
 HIGH = lax.Precision.HIGHEST
+
+
+def state_launch(a0, named_axis):
+    dev_count = jax.lax.axis_size(named_axis)
+    shelf = [a0]
+    for kk in [*range(1, dev_count)]:
+        tile_out = jax.lax.ppermute(
+            shelf[kk - 1], named_axis, [(i0, (i0 - 1) % dev_count) for i0 in range(dev_count)]
+        )
+        shelf.append(tile_out)
+    state_next = jnp.concatenate(shelf, axis=0)
+    current_block = jnp.roll(state_next, shift=jax.lax.axis_index(named_axis) * a0.shape[0], axis=0)
+    return current_block
+
+
+point_form = functools.partial(state_launch, named_axis="fs")
 
 
 def block_scan(queries, key_rows, value_rows, log_decay):
@@ -71,7 +88,7 @@
     block_pieces = (
         lax.all_gather(query_matrix, "fs", axis=0, tiled=True),
         lax.all_gather(key_weight, "fs", axis=0, tiled=True),
-        lax.all_gather(value_weight, "fs", axis=0, tiled=True),
+        point_form(value_weight),
     )
     columns = gathered
     queries, key_rows, value_rows = tuple(

time: 617 us -> 580 us (0.940)
  waiting for transfers between devices: 504 us -> 442 us
  starting transfers between devices: 0.53 us -> 13.9 us
  local copies, waits for them, and re-layouts: 22.3 us -> 32.4 us
    all_gather x1 -> x0, waiting for transfers between devices: 42.9 us -> none  [local(): lax.all_gather(value_weight, 'fs', axis=0, tiled=True)]
    ppermute x0 -> x3, waiting for transfers between devices: none -> 38.9 us  [state_launch(): jax.lax.ppermute(shelf[kk - 1], named_axis, [(i0, (i0 - 1) % dev_count) f...]
    all_gather x1, waiting for transfers between devices: 25.7 us -> 0.02 us  [local(): lax.all_gather(query_matrix, 'fs', axis=0, tiled=True)]
    all_gather x1, waiting for transfers between devices: 23.4 us -> 0.01 us  [local(): gathered = lax.all_gather(tokens, 'tp', axis=1, tiled=True)]
    ppermute x0 -> x3, starting transfers between devices: none -> 13.6 us  [state_launch(): jax.lax.ppermute(shelf[kk - 1], named_axis, [(i0, (i0 - 1) % dev_count) f...]
    all_gather x1, waiting for transfers between devices: 25.3 us -> 15.9 us  [local(): lax.all_gather(key_weight, 'fs', axis=0, tiled=True)]
    unnamed x22 -> x23, local copies, waits for them, and re-layouts: 1.24 us -> 8.83 us
    dynamic_slice x0 -> x8, local copies, waits for them, and re-layouts: none -> 7.38 us  [block_scan(): lax.scan(step, start, (queries, key_rows, value_rows, log_decay))]
  transfers between devices with their start and end apart: 10 -> 12, of which waited for: 9 -> 10; matrix products, arithmetic and copies ran while one was open for 9% -> 12% of each run, Pallas kernels for 0% -> 0%
where the time goes in v1:
time: 580 us; the launch traced here: 579 us
  waiting for transfers between devices  442 us (76%)
  matrix products  41.2 us (7%)
  local copies, waits for them, and re-layouts  32.4 us (6%)
  other arithmetic  23.6 us (4%)
  starting transfers between devices  13.9 us (2%)
  between operations  13.4 us (2%)
  blocking collectives  11.7 us (2%)
    all_gather x1, waiting for transfers between devices, local(): lax.all_gather(up_weight, 'fs', axis=0, tiled=True)  151 us
    all_gather x1, waiting for transfers between devices, local(): lax.all_gather(down_weight, 'fs', axis=1, tiled=True)  149 us
    ppermute x3, waiting for transfers between devices, state_launch(): jax.lax.ppermute(shelf[kk - 1], named_axis, [(i0, (i0 - 1) % dev_count) f...  38.9 us
    reduce_scatter x1, waiting for transfers between devices, local(): lax.psum_scatter(mix_terms.astype(jnp.bfloat16), 'tp', scatter_dimension=...  30.1 us
    reduce_scatter x1, waiting for transfers between devices, local(): lax.psum_scatter(down_terms.astype(jnp.bfloat16), 'tp', scatter_dimension...  29.5 us
    all_gather x1, waiting for transfers between devices, local(): normed_rows = lax.all_gather(normed_local, 'tp', axis=1, tiled=True)  21.8 us
    dot_general x1, matrix products, local(): jnp.dot(activation, lax.all_gather(down_weight, 'fs', axis=1, tiled=True)...  16.5 us
    all_gather x1, waiting for transfers between devices, local(): lax.all_gather(key_weight, 'fs', axis=0, tiled=True)  15.9 us
  transfers between devices with their start and end apart: 12, of which 10 were waited for; matrix products, arithmetic and copies ran while one was open for 12% of the time, Pallas kernels for 0%

profile of v1, /device:TPU:0, one launch (start us, length us, event | category | flops | bytes accessed | tf_op | source)
XLA Modules:
  0.0 578.6 jit_solution(9152169955665068302)
XLA Ops:
  6.5 0.7 all-gather.8.cloned.1.call-update
  8.8 5.1 collective-permute-start
  13.9 11.5 %collective-permute-done = bf16[512,512]{1,0:T(8,128)(2,1)S(1)} collective-permute-done((bf16[512,512]{1,0:T(8,128)(2,1)}, bf16[512,512]{1,0:T(8,128)(2,1)S(1)}, u32[]{:S(2)}, u32[]{:S(2)}) %collective-permute-start) | collective-permute-done | bytes 524320 | tf_op jit(solution)/shard_map/ppermute | solution.py:21
  25.4 4.2 collective-permute-start.1
  29.7 10.2 %collective-permute-done.1 = bf16[512,512]{1,0:T(8,128)(2,1)S(1)} collective-permute-done((bf16[512,512]{1,0:T(8,128)(2,1)S(1)}, bf16[512,512]{1,0:T(8,128)(2,1)S(1)}, u32[]{:S(2)}, u32[]{:S(2)}) %collective-permute-start.1) | collective-permute-done | bytes 524320 | tf_op jit(solution)/shard_map/ppermute | solution.py:21
  39.9 4.3 collective-permute-start.2
  44.9 0.8 dynamic_slice.25
  45.6 1.9 constant_dynamic-update-slice_fusion.7
  47.5 0.8 constant_dynamic-update-slice_fusion.6
  48.4 0.8 constant_dynamic-update-slice_fusion.5
  49.2 17.2 %collective-permute-done.2 = bf16[512,512]{1,0:T(8,128)(2,1)} collective-permute-done((bf16[512,512]{1,0:T(8,128)(2,1)S(1)}, bf16[512,512]{1,0:T(8,128)(2,1)}, u32[]{:S(2)}, u32[]{:S(2)}) %collective-permute-start.2) | collective-permute-done | bytes 524320 | tf_op jit(solution)/shard_map/ppermute | solution.py:21
  66.4 1.9 constant_dynamic-update-slice_fusion.4
  68.3 0.8 constant_dynamic-update-slice_fusion.3
  69.1 0.8 constant_dynamic-update-slice_fusion.2
  69.9 0.8 constant_dynamic-update-slice_fusion.1
  70.8 1.9 constant_dynamic-update-slice_fusion
  72.7 4.5 fusion.24
  77.2 1.6 copy.49
  78.7 1.6 reshape.85
  80.4 3.0 fusion.35
  83.7 2.6 fusion.30
  86.5 15.9 %all-gather.10.cloned.1.call-done = bf16[2048,256]{1,0:T(8,128)(2,1)} async-done(((bf16[512,256]{1,0:T(8,128)(2,1)}), bf16[2048,256]{1,0:T(8,128)(2,1)}) %all-gather.10.cloned.1.call-update) | async-done | bytes 1048592 | tf_op jit(solution)/shard_map/all_gather | solution.py:90
  102.4 2.6 fusion.28
  105.3 0.9 copy_bitcast_fusion.3
  106.2 39.3 %while.13 = (s32[]{:T(128)}, f32[2,128,256]{2,1,0:T(8,128)S(1)}, f32[8,2,64,256]{3,2,1,0:T(8,128)S(1)}, f32[8,2,64,128]{3,2,1,0:T(8,128)S(1)}, f32[8,2,64,128]{3...) while((s32[]{:T(128)}, f32[2,128,256]{2,1,0:T(8,128)S(1)}, ...), condition=%wide.region_3.4_spmd.clone, body=%wide.region_0.3_spmd.clone.sunk | while | flops 132444160 | bytes 2799748 | solution.py:53
  106.2 0.8 dynamic-slice_bitcast_fusion.6
  107.2 1.9 multiply_reduce_fusion.5
  109.4 0.9 constant_dynamic-slice_fusion.2
  111.1 0.9 dynamic-slice_bitcast_fusion.6
  112.1 1.9 multiply_reduce_fusion.5
  114.4 0.9 constant_dynamic-slice_fusion.2
  116.0 0.9 dynamic-slice_bitcast_fusion.6
  117.0 1.9 multiply_reduce_fusion.5
  119.3 0.9 constant_dynamic-slice_fusion.2
  120.9 0.9 dynamic-slice_bitcast_fusion.6
  121.9 1.9 multiply_reduce_fusion.5
  124.2 0.9 constant_dynamic-slice_fusion.2
  125.8 0.9 dynamic-slice_bitcast_fusion.6
  126.8 1.9 multiply_reduce_fusion.5
  129.1 0.9 constant_dynamic-slice_fusion.2
  130.8 0.9 dynamic-slice_bitcast_fusion.6
  131.7 1.9 multiply_reduce_fusion.5
  134.0 0.9 constant_dynamic-slice_fusion.2
  135.7 0.9 dynamic-slice_bitcast_fusion.6
  136.7 1.9 multiply_reduce_fusion.5
  138.9 0.9 constant_dynamic-slice_fusion.2
  140.6 0.9 dynamic-slice_bitcast_fusion.6
  141.6 1.9 multiply_reduce_fusion.5
  143.8 0.9 constant_dynamic-slice_fusion.2
  146.6 0.8 copy.52
  147.5 1.4 all-gather.14.cloned.1.call-done
  148.9 4.2 convolution_convert_fusion.1
  153.2 30.1 %reduce-scatter.3.cloned.1.call-done = bf16[512,512]{1,0:T(8,128)(2,1)} async-done(((bf16[512,2048]{1,0:T(8,128)(2,1)}), bf16[512,512]{1,0:T(8,128)(2,1)}) %reduce-scatter.3.cloned.1.call-update) | async-done | bytes 524304 | tf_op jit(solution)/shard_map/reduce_scatter | solution.py:138
  183.3 1.4 fusion.31
  184.7 5.9 %all-reduce.1 = (f32[512]{0:T(512)S(1)}, f32[512]{0:T(512)S(1)}) all-reduce(f32[512]{0:T(512)S(1)} %get-tuple-element.112, f32[512]{0:T(512)S(1)} %get-tuple-element.111), channel_id=1, replica_groups=mesh['grp'=2,'fs'=4,'tp'=4] {'tp'}, use_global_device_ids=true, to_apply=%region_9.10 | all-reduce | flops 1024 | bytes 8192 | tf_op jit(solution)/shard_map/psum | solution.py:58
  190.7 2.1 multiply_convert_fusion.2
  194.4 21.8 %all-gather.16.cloned.1.call-done = bf16[512,2048]{1,0:T(8,128)(2,1)} async-done(((bf16[512,512]{1,0:T(8,128)(2,1)}), bf16[512,2048]{1,0:T(8,128)(2,1)}) %all-gather.16.cloned.1.call-update) | async-done | bytes 2097168 | tf_op jit(solution)/shard_map/all_gather | solution.py:142
  216.1 151.2 %all-gather.18.cloned.1.call-done = bf16[2048,2048]{1,0:T(8,128)(2,1)} async-done(((bf16[512,2048]{1,0:T(8,128)(2,1)}), bf16[2048,2048]{1,0:T(8,128)(2,1)}) %all-gather.18.cloned.1.call-update) | async-done | bytes 8388624 | tf_op jit(solution)/shard_map/all_gather | solution.py:146
  367.4 149.4 %all-gather.20.cloned.1.call-done = bf16[2048,2048]{1,0:T(8,128)(2,1)} async-done(((bf16[2048,512]{1,0:T(8,128)(2,1)}), bf16[2048,2048]{1,0:T(8,128)(2,1)}) %all-gather.20.cloned.1.call-update) | async-done | bytes 8388624 | tf_op jit(solution)/shard_map/all_gather | solution.py:152
  516.8 16.5 %convolution_convert_fusion = bf16[512,2048]{1,0:T(8,128)(2,1)} fusion(bf16[2048,2048]{1,0:T(8,128)(2,1)} %all-gather.20.cloned.1.call-done, bf16[512,2048]{1,0:T(8,128)(2,1)} %all-gather.16.cloned.1.call-done, bf16[2048,2048]{1,0:T(8,128)(2,1)} %all-gather.18.cloned.1.call-done), kind=kOutput, calls=%fused_computation.25 | convolution fusion | flops 8594128896 | bytes 20971520 | tf_op jit(solution)/shard_map/dot_general | solution.py:150
  533.3 29.5 %reduce-scatter.5.cloned.1.call-done = bf16[512,512]{1,0:T(8,128)(2,1)} async-done(((bf16[512,2048]{1,0:T(8,128)(2,1)}), bf16[512,512]{1,0:T(8,128)(2,1)}) %reduce-scatter.5.cloned.1.call-update) | async-done | bytes 524304 | tf_op jit(solution)/shard_map/reduce_scatter | solution.py:155
  562.8 1.4 fusion.32
  564.2 5.8 all-reduce
  570.0 2.1 multiply_convert_fusion.1
  (111 shorter events, 14.8 us)
Async XLA Ops:
  6.5 73.8 %copy-start = (bf16[2048,32]{0,1:T(8,128)(2,1)S(1)}, bf16[2048,32]{0,1:T(8,128)(2,1)}, u32[]{:S(2)}) copy-start(bf16[2048,32]{0,1:T(8,128)(2,1)} %param.20) | copy-start | bytes 393220
  6.5 61.7 %copy-start.3 = (bf16[512,512]{1,0:T(8,128)(2,1)S(1)}, bf16[512,512]{1,0:T(8,128)(2,1)}, u32[]{:S(2)}) copy-start(bf16[512,512]{1,0:T(8,128)(2,1)} %param.19) | copy-start | bytes 1572868
  6.5 66.1 %all-gather.8.cloned.1.call-start = ((), (), s32[]{:S(2)}) async-start(), calls=%async_computation.2 | async-start | bytes 2621440 | tf_op jit(solution)/shard_map/all_gather | solution.py:83
  7.3 76.4 %all-gather.12.cloned.1.call-start = ((), (), s32[]{:S(2)}) async-start(), calls=%async_computation.4 | async-start | bytes 1310720 | tf_op jit(solution)/shard_map/all_gather | solution.py:89
  8.0 94.4 %all-gather.10.cloned.1.call-start = ((), (), s32[]{:S(2)}) async-start(), calls=%async_computation.3 | async-start | bytes 1310720 | tf_op jit(solution)/shard_map/all_gather | solution.py:90
  8.7 140.2 %all-gather.14.cloned.1.call-start = ((), (), s32[]{:S(2)}) async-start(), calls=%async_computation.5 | async-start | bytes 2621440 | tf_op jit(solution)/shard_map/all_gather | solution.py:135
  8.8 16.6 %collective-permute-start = (bf16[512,512]{1,0:T(8,128)(2,1)}, bf16[512,512]{1,0:T(8,128)(2,1)S(1)}, u32[]{:S(2)}, u32[]{:S(2)}) collective-permute-start(bf16[512,512]{1,0:T(8,128)(2,1)} %param.19), channel_id=1, source_target_pairs={{0,12},{4,0},{8,4},{12,8},{1,13},{5,1},{9,5},{13,9},{2,14},{6,2},{... | collective-permute-start | bytes 1572872 | tf_op jit(solution)/shard_map/ppermute | solution.py:21
  25.4 14.5 %collective-permute-start.1 = (bf16[512,512]{1,0:T(8,128)(2,1)S(1)}, bf16[512,512]{1,0:T(8,128)(2,1)S(1)}, u32[]{:S(2)}, u32[]{:S(2)}) collective-permute-start(bf16[512,512]{1,0:T(8,128)(2,1)S(1)} %collective-permute-done), channel_id=1, source_target_pairs={{0,12},{4,0},{8,4},{12,8},{1,13},{5,1},{9,5},{13,9},{2,14},{6,2},{... | collective-permute-start | bytes 1572872 | tf_op jit(solution)/shard_map/ppermute | solution.py:21
  29.6 153.7 %reduce-scatter.3.cloned.1.call-start = ((), (), s32[]{:S(2)}) async-start(), calls=%async_computation.6 | async-start | bytes 2621440 | tf_op jit(solution)/shard_map/reduce_scatter | solution.py:138
  39.9 26.4 %collective-permute-start.2 = (bf16[512,512]{1,0:T(8,128)(2,1)S(1)}, bf16[512,512]{1,0:T(8,128)(2,1)}, u32[]{:S(2)}, u32[]{:S(2)}) collective-permute-start(bf16[512,512]{1,0:T(8,128)(2,1)S(1)} %collective-permute-done.1), channel_id=1, source_target_pairs={{0,12},{4,0},{8,4},{12,8},{1,13},{5,1},{9,5},{13,9},{2,14},{6,2},{... | collective-permute-start | bytes 1572872 | tf_op jit(solution)/shard_map/ppermute | solution.py:21
  148.9 34.4 %copy-start.2 = (bf16[512,512]{1,0:T(8,128)(2,1)S(1)}, bf16[512,512]{1,0:T(8,128)(2,1)}, u32[]{:S(2)}) copy-start(bf16[512,512]{1,0:T(8,128)(2,1)} %param.16) | copy-start | bytes 1572868
  148.9 41.8 %copy-start.4 = (f32[512]{0:T(512)S(1)}, f32[512]{0:T(512)}, u32[]{:S(2)}) copy-start(f32[512]{0:T(512)} %param.26) | copy-start | bytes 6148
  153.2 63.0 %all-gather.16.cloned.1.call-start = ((), (), s32[]{:S(2)}) async-start(), calls=%async_computation.7 | async-start | bytes 2621440 | tf_op jit(solution)/shard_map/all_gather | solution.py:142
  192.8 174.6 %all-gather.18.cloned.1.call-start = ((), (), s32[]{:S(2)}) async-start(), calls=%async_computation.8 | async-start | bytes 10485760 | tf_op jit(solution)/shard_map/all_gather | solution.py:146
  193.5 323.2 %all-gather.20.cloned.1.call-start = ((), (), s32[]{:S(2)}) async-start(), calls=%async_computation.9 | async-start | bytes 10485760 | tf_op jit(solution)/shard_map/all_gather | solution.py:152
  194.3 368.5 %copy-start.1 = (bf16[512,512]{1,0:T(8,128)(2,1)S(1)}, bf16[512,512]{1,0:T(8,128)(2,1)}, u32[]{:S(2)}) copy-start(bf16[512,512]{1,0:T(8,128)(2,1)} %multiply_convert_fusion.2) | copy-start | bytes 1572868
  194.3 375.6 %copy-start.5 = (f32[512]{0:T(512)S(1)}, f32[512]{0:T(512)}, u32[]{:S(2)}) copy-start(f32[512]{0:T(512)} %param.29) | copy-start | bytes 6148
  194.3 368.5 %reduce-scatter.5.cloned.1.call-start = ((), (), s32[]{:S(2)}) async-start(), calls=%async_computation.10 | async-start | bytes 2621440 | tf_op jit(solution)/shard_map/reduce_scatter | solution.py:155
Sparse Core Ops, SparseCore 0:
  8.9 25.2 all-gather.7
  35.8 34.8 all-gather.11
  72.2 30.1 all-gather.9
  103.8 45.0 all-gather.13
  153.3 29.9 reduce-scatter.2
  192.9 23.1 all-gather.15
  217.7 149.6 all-gather.17
  368.9 147.7 all-gather.19
  533.4 29.3 reduce-scatter.4
